TPU v7x, 32 devices: a whole 2x2x4 slice. The times are simulated.
32 devices in a mesh: grp: 2 (over x), ep: 16 (over z, y, core).
Axes of the slice: x: 2, y: 2, z: 4, core: 2. Of those that a mesh axis runs over, the one named last changes fastest.
Arguments:
- tokens: bfloat16 [128, 2048], P(('grp', 'ep')), parts along dimension 0, may hold values from -6 to 6
- lengths: int32 [128], P(('grp', 'ep')), parts along dimension 0, may hold values from 128 to 1024, as said below
- cache_key: bfloat16 [128, 1024, 256], P(('grp', 'ep')), parts along dimension 0, may hold values from -6 to 6
- cache_value: bfloat16 [128, 1024, 256], P(('grp', 'ep')), parts along dimension 0, may hold values from -6 to 6
- routes: int32 [128, 2], P(('grp', 'ep')), parts along dimension 0, may hold values from 0 to 3, all different within a row
- route_logits: float32 [128, 2], P(('grp', 'ep')), parts along dimension 0, may hold values from -6 to 6
- mix_gain: float32 [2048], replicated, may hold values from 0.1 to 1.9
- query_gain: float32 [64], replicated, may hold values from 0.1 to 1.9
- key_gain: float32 [64], replicated, may hold values from 0.1 to 1.9
- head_bias: float32 [16], replicated, may hold values from -9 to -3.5
- w_query: bfloat16 [2048, 1024], P('ep'), may hold values from -0.125 to 0.125
- w_key: bfloat16 [2048, 256], P('ep'), may hold values from -0.125 to 0.125
- w_value: bfloat16 [2048, 256], P('ep'), may hold values from -0.125 to 0.125
- w_out: bfloat16 [1024, 2048], P(None, 'ep'), may hold values from -0.1875 to 0.1875
- ffn_gain: float32 [2048], replicated, may hold values from 0.1 to 1.9
- w_gate: bfloat16 [2048, 28672], P(None, 'ep'), may hold values from -0.125 to 0.125
- w_up: bfloat16 [2048, 28672], P(None, 'ep'), may hold values from -0.125 to 0.125
- w_down: bfloat16 [28672, 2048], P('ep'), may hold values from -0.0625 to 0.0625
Outputs:
- output: bfloat16 [128, 2048], P(('grp', 'ep')), parts along dimension 0
- new_key: bfloat16 [128, 256], P(('grp', 'ep')), parts along dimension 0
- new_value: bfloat16 [128, 256], P(('grp', 'ep')), parts along dimension 0
There are 2 independent parts, one for each index of `grp`. A program takes and returns all parts, laid end to end along the dimension named above; an argument that names none is the same for every part. Nothing has to cross between parts.
Inputs may be any that keep to these rules, and one draw needn't show every extreme that they name: `lengths`: some sequence has all 1024 positions live.
All inputs are finite; a program needn't handle non-finite values.
Results may differ from a plain program's by a relative error of at most 0.0085.
Values may be sent and summed in bfloat16 or wider, within the bound.
A program may use at most 128 MiB of HBM per device.

v0:
```python
import jax
import jax.numpy as jnp
from jax import lax
from jax.sharding import PartitionSpec as P

HEADS = 16
KV_HEADS = 4
HEAD_DIM = 64
FF = 7168
EXPERTS = 4


EPSILON = 1e-06


def rms_scaled(values, gain):
    return values * lax.rsqrt(jnp.mean(values * values, axis=-1, keepdims=True) + EPSILON) * gain


def route_weights(routes, route_logits):
    experts_iota = jnp.arange(EXPERTS, dtype=jnp.int32)[None, :]
    first_share = jax.nn.sigmoid(route_logits[:, 0:1] - route_logits[:, 1:2])
    second_share = jax.nn.sigmoid(route_logits[:, 1:2] - route_logits[:, 0:1])
    return jnp.where(routes[:, 0:1] == experts_iota, first_share, 0.0) + jnp.where(
        routes[:, 1:2] == experts_iota, second_share, 0.0
    )


def stick_attend(queries, lengths, cache_key, cache_value, query_gain, head_bias):
    batch_rows = queries.shape[0]
    cache_len = cache_key.shape[1]
    group_size = HEADS // KV_HEADS
    normed_query = rms_scaled(queries.reshape(batch_rows, HEADS, HEAD_DIM), query_gain).astype(
        jnp.bfloat16
    )
    normed_query = normed_query.reshape(batch_rows, KV_HEADS, group_size, HEAD_DIM)
    key_heads = cache_key.reshape(batch_rows, cache_len, KV_HEADS, HEAD_DIM)
    value_heads = cache_value.reshape(batch_rows, cache_len, KV_HEADS, HEAD_DIM)
    scores = jnp.einsum(
        "bkgd,blkd->bkgl", normed_query, key_heads, preferred_element_type=jnp.float32
    ) * HEAD_DIM ** (-0.5)
    scores = scores + head_bias.reshape(KV_HEADS, group_size)[None, :, :, None]
    live_mask = (
        jnp.arange(cache_len, dtype=jnp.int32)[None, None, None, :] < lengths[:, None, None, None]
    )
    remain = jnp.where(live_mask, jax.nn.log_sigmoid(-scores), 0.0)
    after_sum = lax.cumsum(remain, axis=3, reverse=True) - remain
    weights = jnp.where(live_mask, jnp.exp(jax.nn.log_sigmoid(scores) + after_sum), 0.0).astype(
        jnp.bfloat16
    )
    attended = jnp.einsum(
        "bkgl,blkd->bkgd", weights, value_heads, preferred_element_type=jnp.float32
    )
    return attended.reshape(batch_rows, HEADS * HEAD_DIM).astype(jnp.bfloat16)


def local(
    tokens,
    lengths,
    cache_key,
    cache_value,
    routes,
    route_logits,
    mix_gain,
    query_gain,
    key_gain,
    head_bias,
    w_query,
    w_key,
    w_value,
    w_out,
    ffn_gain,
    w_gate,
    w_up,
    w_down,
):
    token_rows = tokens.shape[0]
    key_width = w_key.shape[1]
    as_float = tokens.astype(jnp.float32)
    normed = rms_scaled(as_float, mix_gain).astype(jnp.bfloat16)
    pieces = (
        lax.all_gather(w_query, "ep", axis=0, tiled=True),
        lax.all_gather(w_key, "ep", axis=0, tiled=True),
        lax.all_gather(w_value, "ep", axis=0, tiled=True),
    )
    queries, fresh_key, fresh_value = tuple(
        (jnp.dot(normed, weight, preferred_element_type=jnp.float32) for weight in pieces)
    )
    new_key = rms_scaled(fresh_key.reshape(token_rows, KV_HEADS, HEAD_DIM), key_gain)
    new_key = new_key.reshape(token_rows, key_width).astype(jnp.bfloat16)
    new_value = fresh_value.astype(jnp.bfloat16)
    attended = stick_attend(queries, lengths, cache_key, cache_value, query_gain, head_bias)
    mixed = as_float + jnp.dot(
        attended,
        lax.all_gather(w_out, "ep", axis=1, tiled=True),
        preferred_element_type=jnp.float32,
    )
    expert_in = rms_scaled(mixed, ffn_gain).astype(jnp.bfloat16)
    every_gate = lax.all_gather(route_weights(routes, route_logits), "ep", axis=0, tiled=True)
    ff_share = w_gate.shape[1]
    my_expert = lax.axis_index("ep") // (FF // ff_share)
    my_gate = lax.dynamic_slice_in_dim(every_gate, my_expert, 1, 1)
    input_rows = lax.all_gather(expert_in, "ep", axis=0, tiled=True)
    gate_value = jnp.dot(input_rows, w_gate, preferred_element_type=jnp.float32)
    up_value = jnp.dot(input_rows, w_up, preferred_element_type=jnp.float32)
    hidden = (jax.nn.silu(gate_value) * up_value * my_gate).astype(jnp.bfloat16)
    expert_sum = lax.psum_scatter(
        jnp.dot(hidden, w_down, preferred_element_type=jnp.float32),
        "ep",
        scatter_dimension=0,
        tiled=True,
    )
    return ((mixed + expert_sum).astype(jnp.bfloat16), new_key, new_value)


def solution(mesh):
    return jax.shard_map(
        local,
        mesh=mesh,
        in_specs=(
            P(("grp", "ep"), None),
            P(("grp", "ep")),
            P(("grp", "ep"), None, None),
            P(("grp", "ep"), None, None),
            P(("grp", "ep"), None),
            P(("grp", "ep"), None),
            P(),
            P(),
            P(),
            P(),
            P("ep", None),
            P("ep", None),
            P("ep", None),
            P(None, "ep"),
            P(),
            P(None, "ep"),
            P(None, "ep"),
            P("ep", None),
        ),
        out_specs=(P(("grp", "ep"), None), P(("grp", "ep"), None), P(("grp", "ep"), None)),
        check_vma=False,
    )
```

profile of v0, /device:TPU:0, one launch (start us, length us, event | category | flops | bytes accessed | tf_op | source)
XLA Modules:
  0.0 323.6 jit_solution(14233699592130676212)
XLA Ops:
  7.2 0.7 all-gather.11.cloned.1.call-update
  8.0 0.7 all-gather.7.cloned.1.call-update
  10.1 0.8 slice_bitcast_fusion.1
  10.8 0.8 divide_bitcast_fusion.1
  11.6 23.2 %all-gather.1 = f32[16,4,4]{2,1,0:T(4,128)S(1)} all-gather(f32[1,4,4]{2,1,0:T(4,128)S(1)} %add_bitcast_fusion), channel_id=1, replica_groups=mesh['grp'=2,'ep'=16] {'ep'}, dimensions={0}, use_global_device_ids=true | all-gather | bytes 1088 | tf_op jit(solution)/shard_map/all_gather | solution.py:99
  35.0 0.9 fusion.21
  35.9 0.7 iota_compare_fusion
  36.6 4.0 %copy.27 = bf16[4,1024,256]{1,2,0:T(8,128)(2,1)} copy(bf16[4,1024,256]{2,1,0:T(8,128)(2,1)} %param.20) | data formatting | bytes 4194304 | tf_op args[2]
  40.7 2.6 copy.28
  44.6 6.3 %all-gather.11.cloned.1.call-done = bf16[2048,256]{1,0:T(8,128)(2,1)} async-done(((bf16[128,256]{1,0:T(8,128)(2,1)}), bf16[2048,256]{1,0:T(8,128)(2,1)}) %all-gather.11.cloned.1.call-update) | async-done | bytes 1048592 | tf_op jit(solution)/shard_map/all_gather | solution.py:83
  50.8 1.5 fusion.37
  52.7 49.7 %all-gather.7.cloned.1.call-done = bf16[2048,1024]{1,0:T(8,128)(2,1)} async-done(((bf16[128,1024]{1,0:T(8,128)(2,1)}), bf16[2048,1024]{1,0:T(8,128)(2,1)}) %all-gather.7.cloned.1.call-update) | async-done | bytes 4194320 | tf_op jit(solution)/shard_map/all_gather | solution.py:82
  102.4 2.9 fusion.36
  105.6 2.2 fusion.15
  108.0 79.2 %reduce-window.6 = f32[4,4,4,8,128]{4,3,2,1,0:T(8,128)S(1)} reduce-window(f32[4,4,4,8,128]{4,3,2,1,0:T(8,128)S(1)} %reshape.103, f32[]{:T(128)} %constant.36.clone.1), window={size=1x1x1x1x128 pad=0_0x0_0x0_0x0_0x0_127}, to_apply=%region_2.0 | reduce-window | flops 8323072 | bytes 524292 | tf_op jit(solution)/shard_map/reduce-window
  187.4 2.8 reduce-window.9
  190.6 0.9 convolution_convert_fusion
  191.6 3.0 multiply_reduce_fusion
  194.7 19.6 %all-gather = bf16[16,4,2048]{2,1,0:T(4,128)(2,1)S(1)} all-gather(bf16[1,4,2048]{2,1,0:T(4,128)(2,1)S(1)} %fusion.25), channel_id=1, replica_groups=mesh['grp'=2,'ep'=16] {'ep'}, dimensions={0}, use_global_device_ids=true | all-gather | bytes 278528 | tf_op jit(solution)/shard_map/all_gather | solution.py:103
  214.4 4.4 %fusion.38 = f32[64,1792]{1,0:T(8,128)S(1)} fusion(bf16[64,2048]{1,0:T(8,128)(2,1)S(1)} %reshape.107, bf16[2048,1792]{1,0:T(8,128)(2,1)} %param.33), kind=kOutput, calls=%fused_computation.62 | convolution fusion | flops 469762048 | bytes 8060928 | tf_op jit(solution)/shard_map/dot_general | solution.py:104
  218.8 8.7 %fusion.3 = f32[64,2048]{1,0:T(8,128)} fusion(bf16[1792,2048]{1,0:T(8,128)(2,1)} %param.35, bf16[64,2048]{1,0:T(8,128)(2,1)S(1)} %reshape.107, bf16[2048,1792]{1,0:T(8,128)(2,1)} %param.34, f32[64,1792]{1,0:T(8,128)S(1)} %fusion.38, f32[64]{0:T(128)S(1)} %bitcast.34), kind=kOutput, calls=%fused_computation.8 | convolution fusion | flops 940326912 | bytes 15925504 | tf_op jit(solution)/shard_map/dot_general | solution.py:108
  228.1 2.1 convolution_convert_fusion.1
  230.2 85.5 %all-reduce.3.cloned.1.call-done = f32[64,2048]{1,0:T(8,128)} async-done(((f32[64,2048]{1,0:T(8,128)}), f32[64,2048]{1,0:T(8,128)}) %all-reduce.3.cloned.1.call-update) | async-done | bytes 524304
  315.7 1.5 fusion.24
  (56 shorter events, 4.6 us)
Async XLA Ops:
  7.2 33.4 %copy-start.5 = (f32[16]{0:T(128)S(1)}, f32[16]{0:T(128)}, u32[]{:S(2)}) copy-start(f32[16]{0:T(128)} %param.27) | copy-start | bytes 196
  7.2 33.5 %copy-start = (bf16[4,1024,256]{2,1,0:T(8,128)(2,1)S(1)}, bf16[4,1024,256]{2,1,0:T(8,128)(2,1)}, u32[]{:S(2)}) copy-start(bf16[4,1024,256]{2,1,0:T(8,128)(2,1)} %param.21) | copy-start | bytes 6291460
  7.2 43.6 %all-gather.11.cloned.1.call-start = ((), (), s32[]{:S(2)}) async-start(), calls=%async_computation.2 | async-start | bytes 1114112 | tf_op jit(solution)/shard_map/all_gather | solution.py:83
  7.9 94.5 %all-gather.7.cloned.1.call-start = ((), (), s32[]{:S(2)}) async-start(), calls=%async_computation | async-start | bytes 4456448 | tf_op jit(solution)/shard_map/all_gather | solution.py:82
  8.7 182.9 %all-gather.9.cloned.1.call-start = ((), (), s32[]{:S(2)}) async-start(), calls=%async_computation.1 | async-start | bytes 4456448 | tf_op jit(solution)/shard_map/all_gather | solution.py:95
  9.4 218.7 %all-gather.13.cloned.1.call-start = ((), (), s32[]{:S(2)}) async-start(), calls=%async_computation.3 | async-start | bytes 1114112 | tf_op jit(solution)/shard_map/all_gather | solution.py:84
  10.0 305.7 %all-reduce.3.cloned.1.call-start = ((), (), s32[]{:S(2)}) async-start(), calls=%async_computation.4 | async-start | bytes 1048576
  36.6 6.7 %copy-start.6 = (f32[64]{0:T(128)S(1)}, f32[64]{0:T(128)}, u32[]{:S(2)}) copy-start(f32[64]{0:T(128)} %param.26) | copy-start | bytes 772
  36.6 6.7 %copy-start.8 = (u32[32]{0:T(128)S(1)}, u32[32]{0:T(128)}, u32[]{:S(2)}) copy-start(u32[32]{0:T(128)} %constant.57) | copy-start | bytes 388
  36.6 14.2 %copy-start.2 = (bf16[4,2048]{1,0:T(4,128)(2,1)S(1)}, bf16[4,2048]{1,0:T(4,128)(2,1)}, u32[]{:S(2)}) copy-start(bf16[4,2048]{1,0:T(4,128)(2,1)} %param.18) | copy-start | bytes 49156
  36.6 14.2 %copy-start.3 = (f32[2048]{0:T(1024)S(1)}, f32[2048]{0:T(1024)}, u32[]{:S(2)}) copy-start(f32[2048]{0:T(1024)} %param.24) | copy-start | bytes 24580
  40.7 64.9 %copy-start.7 = (f32[64]{0:T(128)S(1)}, f32[64]{0:T(128)}, u32[]{:S(2)}) copy-start(f32[64]{0:T(128)} %param.25) | copy-start | bytes 772
  52.7 137.9 %copy-start.1 = (bf16[4,1024,256]{1,2,0:T(8,128)(2,1)S(1)}, bf16[4,1024,256]{1,2,0:T(8,128)(2,1)}, u32[]{:S(2)}) copy-start(bf16[4,1024,256]{1,2,0:T(8,128)(2,1)} %copy.28) | copy-start | bytes 6291460
  190.6 4.1 %copy-start.4 = (f32[2048]{0:T(1024)S(1)}, f32[2048]{0:T(1024)}, u32[]{:S(2)}) copy-start(f32[2048]{0:T(1024)} %param.32) | copy-start | bytes 24580
Sparse Core Ops, SparseCore 0:
  10.2 40.6 all-gather.10
  53.0 49.3 all-gather.6
  104.5 50.9 all-gather.8
  157.6 36.2 all-gather.12
  227.7 87.9 all-reduce.2
where the time goes:
time: 324 us
  waiting for transfers between devices  144 us (44%)
  other arithmetic  87 us (27%)
  blocking collectives  42.8 us (13%)
  matrix products  25.7 us (8%)
  between operations  14.6 us (5%)
  local copies, waits for them, and re-layouts  9.35 us (3%)
    unnamed x6, waiting for transfers between devices  88 us
    another operation x2, other arithmetic  82.1 us
    all_gather x1, waiting for transfers between devices, local(): lax.all_gather(w_query, 'ep', axis=0, tiled=True)  49.7 us
    all_gather x1, blocking collectives, local(): lax.all_gather(route_weights(routes, route_logits), 'ep', axis=0, tiled=T...  23.2 us
    all_gather x1, blocking collectives, local(): input_rows = lax.all_gather(expert_in, 'ep', axis=0, tiled=True)  19.6 us
    dot_general x1, matrix products, local(): jnp.dot(hidden, w_down, preferred_element_type=jnp.float32)  8.67 us
    unnamed x23, local copies, waits for them, and re-layouts  7.29 us
  transfers between devices with their start and end apart: 5, of which 3 were waited for; matrix products, arithmetic and copies ran while one was open for 37% of the time, Pallas kernels for 0%

commit v1 on v0

--- a/solution.py
+++ b/solution.py
@@ -1,6 +1,10 @@
+import functools
+
 import jax
 import jax.numpy as jnp
 from jax import lax
+from jax.experimental import pallas as pl
+from jax.experimental.pallas import tpu as pltpu
 from jax.sharding import PartitionSpec as P
 
 HEADS = 16
@@ -54,7 +58,7 @@
     return attended.reshape(batch_rows, HEADS * HEAD_DIM).astype(jnp.bfloat16)
 
 
-def local(
+def plain(
     tokens,
     lengths,
     cache_key,
@@ -113,9 +117,483 @@
     return ((mixed + expert_sum).astype(jnp.bfloat16), new_key, new_value)
 
 
+WEIGHT_PARTS = 4
+DOWN_PARTS = 4
+COLUMNS = 256
+
+
+def dot(left, right):
+    return jnp.dot(left, right, preferred_element_type=jnp.float32)
+
+
+def iota(shape, dim):
+    return lax.broadcasted_iota(jnp.int32, shape, dim)
+
+
+def fused(
+    n,
+    tokens_ref,
+    lengths_ref,
+    ck_hbm,
+    cv_hbm,
+    routes_ref,
+    logits_ref,
+    mix_gain_ref,
+    query_gain_ref,
+    key_gain_ref,
+    head_bias_ref,
+    wq_hbm,
+    wk_hbm,
+    wv_hbm,
+    wo_hbm,
+    ffn_gain_ref,
+    wg_hbm,
+    wu_hbm,
+    wd_hbm,
+    out_ref,
+    new_key_ref,
+    new_value_ref,
+    wq,
+    wk,
+    wv,
+    wo,
+    ck,
+    cv,
+    wg,
+    wu,
+    wd,
+    s1,
+    r1,
+    s2,
+    r2,
+    r3,
+    r4,
+    s5,
+    r5,
+    token_cols,
+    aux_rows,
+    attended_rows,
+    expert_in,
+    hidden,
+    small_sem,
+    key_sem,
+    value_sem,
+    weight_sem,
+    send_sem,
+    recv_sem,
+):
+    me = lax.axis_index("ep")
+    rows, width = tokens_ref.shape
+    all_rows = rows * n
+    share = width // n
+    q_width = wq.shape[1]
+    k_width = wk.shape[1]
+    cache_len = ck.shape[1]
+    group_size = HEADS // KV_HEADS
+    ff_share = wg.shape[1]
+    my_expert = me // (FF // ff_share)
+
+    barrier = pltpu.get_barrier_semaphore()
+    for d in range(1, n):
+        pl.semaphore_signal(
+            barrier,
+            inc=1,
+            device_id={"ep": lax.rem(me + d, n)},
+            device_id_type=pl.DeviceIdType.MESH,
+        )
+
+    small = [
+        pltpu.make_async_copy(a, b, small_sem.at[i])
+        for i, (a, b) in enumerate(((wq_hbm, wq), (wk_hbm, wk), (wv_hbm, wv), (wo_hbm, wo)))
+    ]
+    for c in small[:3]:
+        c.start()
+    keys = [pltpu.make_async_copy(ck_hbm.at[b], ck.at[b], key_sem.at[b]) for b in range(rows)]
+    values = [pltpu.make_async_copy(cv_hbm.at[b], cv.at[b], value_sem.at[b]) for b in range(rows)]
+    for c in keys + values + small[3:]:
+        c.start()
+    weights = []
+    for which, (a, b) in enumerate(((wg_hbm, wg), (wu_hbm, wu), (wd_hbm, wd))):
+        step = b.shape[0] // WEIGHT_PARTS
+        for part in range(WEIGHT_PARTS):
+            piece = pl.ds(part * step, step)
+            weights.append(
+                pltpu.make_async_copy(
+                    a.at[piece], b.at[piece], weight_sem.at[which, part]
+                )
+            )
+    for c in weights:
+        c.start()
+
+    sent = []
+
+    def send(stage, d, source, target):
+        copy = pltpu.make_async_remote_copy(
+            src_ref=source,
+            dst_ref=target,
+            send_sem=send_sem.at[stage, d],
+            recv_sem=recv_sem.at[stage, me],
+            device_id={"ep": lax.rem(me + d, n)},
+            device_id_type=pl.DeviceIdType.MESH,
+        )
+        copy.start()
+        sent.append(copy)
+
+    def arrive(stage, d, target_of):
+        source = lax.rem(me + d, n)
+        pltpu.make_async_remote_copy(
+            src_ref=target_of(source),
+            dst_ref=target_of(source),
+            send_sem=send_sem.at[stage, d],
+            recv_sem=recv_sem.at[stage, source],
+            device_id={"ep": source},
+            device_id_type=pl.DeviceIdType.MESH,
+        ).wait_recv()
+
+    as_float = tokens_ref[...].astype(jnp.float32)
+    scale = lax.rsqrt(jnp.mean(as_float * as_float, axis=1, keepdims=True) + EPSILON)
+    lane = iota((rows, 128), 1)
+    logit_gap = logits_ref[:, 0:1] - logits_ref[:, 1:2]
+    first_share = 1.0 / (1.0 + jnp.exp(-logit_gap))
+    second_share = 1.0 / (1.0 + jnp.exp(logit_gap))
+    expert_lane = lane % EXPERTS
+    gates = jnp.where(routes_ref[:, 0:1] == expert_lane, first_share, 0.0) + jnp.where(
+        routes_ref[:, 1:2] == expert_lane, second_share, 0.0
+    )
+    aux = jnp.where(lane < 3 * EXPERTS, gates, scale)
+    high = aux.astype(jnp.bfloat16).astype(jnp.float32)
+    middle = (aux - high).astype(jnp.bfloat16).astype(jnp.float32)
+    low = aux - high - middle
+    term = jnp.where(lane < 3 * EXPERTS, lane // EXPERTS, lane - 3 * EXPERTS)
+    aux = jnp.where(term == 0, high, jnp.where(term == 1, middle, low))
+    for peer in range(n):
+        block = jnp.concatenate(
+            [as_float[:, peer * share : (peer + 1) * share], aux], axis=0
+        ).astype(jnp.bfloat16)
+        s1[peer] = block
+    pl.semaphore_wait(barrier, n - 1)
+    for d in range(1, n):
+        send(0, d, s1.at[lax.rem(me + d, n)], r1.at[me])
+    r1[me] = s1[me]
+    for c in small[:3]:
+        c.wait()
+    for d in range(1, n):
+        arrive(0, d, lambda source: r1.at[source])
+    for peer in range(n):
+        block = r1[peer].astype(jnp.float32)
+        token_cols[peer * rows : (peer + 1) * rows, :] = block[:rows]
+        aux_rows[peer * rows : (peer + 1) * rows, :] = block[rows:]
+    aux = aux_rows[...]
+    lane = iota(aux.shape, 1)
+    row_scale = jnp.sum(
+        jnp.where((lane >= 3 * EXPERTS) & (lane < 3 * EXPERTS + 3), aux, 0.0), axis=1, keepdims=True
+    )
+    my_gate = jnp.sum(
+        jnp.where((lane < 3 * EXPERTS) & (lane % EXPERTS == my_expert), aux, 0.0),
+        axis=1,
+        keepdims=True,
+    )
+    my_gain = mix_gain_ref[:, pl.ds(pl.multiple_of(me * share, share), share)]
+    normed = (token_cols[...] * row_scale * my_gain).astype(jnp.bfloat16)
+
+    for weight, start in ((wq, 0), (wk, q_width), (wv, q_width + k_width)):
+        partial = dot(normed, weight[...])
+        for peer in range(n):
+            s2[peer, :, start : start + weight.shape[1]] = partial[
+                peer * rows : (peer + 1) * rows
+            ].astype(jnp.bfloat16)
+    for d in range(1, n):
+        send(1, d, s2.at[lax.rem(me + d, n)], r2.at[me])
+    r2[me] = s2[me]
+
+    head_of_lane = iota((HEADS, q_width), 1) // HEAD_DIM
+    own_lane = head_of_lane == iota((HEADS, q_width), 0)
+    source_lane = iota((q_width, k_width), 0)
+    target_lane = iota((q_width, k_width), 1)
+    fold = jnp.where(
+        (source_lane // (HEAD_DIM * group_size) == target_lane // HEAD_DIM)
+        & (source_lane % HEAD_DIM == target_lane % HEAD_DIM),
+        1.0,
+        0.0,
+    ).astype(jnp.bfloat16)
+    later = jnp.where(
+        iota((COLUMNS, COLUMNS), 0) > iota((COLUMNS, COLUMNS), 1), 1.0, 0.0
+    ).astype(jnp.bfloat16)
+    query_gain = jnp.concatenate([query_gain_ref[...]] * HEADS, axis=1)
+    key_gain = jnp.concatenate([key_gain_ref[...]] * KV_HEADS, axis=1)
+
+    for d in range(1, n):
+        arrive(1, d, lambda source: r2.at[source])
+    total = r2[0].astype(jnp.float32)
+    for peer in range(1, n):
+        total = total + r2[peer].astype(jnp.float32)
+    queries = total[:, :q_width]
+    fresh_key = total[:, q_width : q_width + k_width]
+    new_value_ref[...] = total[:, q_width + k_width :].astype(jnp.bfloat16)
+    squares = fresh_key * fresh_key
+    key_lane = iota(squares.shape, 1) // HEAD_DIM
+    key_scale = jnp.zeros_like(squares)
+    for g in range(KV_HEADS):
+        mean = jnp.sum(jnp.where(key_lane == g, squares, 0.0), axis=1, keepdims=True) / HEAD_DIM
+        key_scale = jnp.where(key_lane == g, lax.rsqrt(mean + EPSILON), key_scale)
+    new_key_ref[...] = (fresh_key * key_scale * key_gain).astype(jnp.bfloat16)
+
+    spread = []
+    for b in range(rows):
+        wide = jnp.where(own_lane, jnp.broadcast_to(queries[b : b + 1], own_lane.shape), 0.0)
+        mean = jnp.sum(wide * wide, axis=1, keepdims=True) / HEAD_DIM
+        spread.append((wide * lax.rsqrt(mean + EPSILON) * query_gain).astype(jnp.bfloat16))
+    folded = dot(jnp.concatenate(spread, axis=0), fold).astype(jnp.bfloat16)
+    blocks = cache_len // COLUMNS
+    position = iota((HEADS, cache_len), 1)
+    own_group = iota((HEADS, k_width), 1) // HEAD_DIM == iota((HEADS, k_width), 0) // group_size
+    heads = []
+    for b in range(rows):
+        keys[b].wait()
+        scores = lax.dot_general(
+            folded[b * HEADS : (b + 1) * HEADS],
+            ck[b],
+            (((1,), (1,)), ((), ())),
+            preferred_element_type=jnp.float32,
+        ) * HEAD_DIM ** (-0.5)
+        scores = scores + head_bias_ref[...]
+        live = position < lengths_ref[b]
+        tail_log = jnp.log1p(jnp.exp(-jnp.abs(scores)))
+        remain = jnp.where(live, jnp.minimum(-scores, 0.0) - tail_log, 0.0)
+        stacked = jnp.concatenate(
+            [remain[:, i * COLUMNS : (i + 1) * COLUMNS] for i in range(blocks)], axis=0
+        )
+        high = stacked.astype(jnp.bfloat16)
+        rest = stacked - high.astype(jnp.float32)
+        middle = rest.astype(jnp.bfloat16)
+        low = (rest - middle.astype(jnp.float32)).astype(jnp.bfloat16)
+        sums = dot(jnp.concatenate([high, middle, low], axis=0), later)
+        count = blocks * HEADS
+        sums = sums[:count] + sums[count : 2 * count] + sums[2 * count :]
+        totals = jnp.sum(stacked, axis=1, keepdims=True)
+        after = [None] * blocks
+        carry = jnp.zeros((HEADS, 1), jnp.float32)
+        for i in reversed(range(blocks)):
+            after[i] = sums[i * HEADS : (i + 1) * HEADS] + carry
+            carry = carry + totals[i * HEADS : (i + 1) * HEADS]
+        after_sum = jnp.concatenate(after, axis=1)
+        chance = jnp.exp(jnp.minimum(scores, 0.0) - tail_log + after_sum)
+        weight = jnp.where(live, chance, 0.0).astype(jnp.bfloat16)
+        values[b].wait()
+        mixed_heads = dot(weight, cv[b])
+        heads.append(jnp.where(own_group, mixed_heads, 0.0).astype(jnp.bfloat16))
+    unfolded = lax.dot_general(
+        jnp.concatenate(heads, axis=0),
+        fold,
+        (((1,), (1,)), ((), ())),
+        preferred_element_type=jnp.float32,
+    )
+    attended = [
+        jnp.sum(
+            jnp.where(own_lane, unfolded[b * HEADS : (b + 1) * HEADS], 0.0), axis=0, keepdims=True
+        )
+        for b in range(rows)
+    ]
+    r3[me] = jnp.concatenate(attended, axis=0).astype(jnp.bfloat16)
+
+    for d in range(1, n):
+        send(2, d, r3.at[me], r3.at[me])
+    small[3].wait()
+    for d in range(1, n):
+        arrive(2, d, lambda source: r3.at[source])
+    for peer in range(n):
+        attended_rows[peer * rows : (peer + 1) * rows, :] = r3[peer].astype(jnp.float32)
+    mixed = token_cols[...] + dot(attended_rows[...].astype(jnp.bfloat16), wo[...])
+    r4[me] = mixed.astype(jnp.bfloat16)
+
+    for d in range(1, n):
+        send(3, d, r4.at[me], r4.at[me])
+    for d in range(1, n):
+        arrive(3, d, lambda source: r4.at[source])
+    squares = jnp.zeros((all_rows, share), jnp.float32)
+    for peer in range(n):
+        block = r4[peer].astype(jnp.float32)
+        squares = squares + block * block
+    scale = lax.rsqrt(jnp.sum(squares, axis=1, keepdims=True) / width + EPSILON)
+    pick = jnp.where(
+        iota((8, all_rows), 1) == iota((8, all_rows), 0) + me * rows, 1.0, 0.0
+    ).astype(jnp.bfloat16)
+    own_mixed = []
+    for peer in range(n):
+        columns = slice(peer * share, (peer + 1) * share)
+        block = r4[peer]
+        own_mixed.append(dot(pick, block)[:rows])
+        expert_in[:, columns] = (
+            block.astype(jnp.float32) * scale * ffn_gain_ref[:, columns]
+        ).astype(jnp.bfloat16)
+    own_mixed = jnp.concatenate(own_mixed, axis=1)
+
+    for c in weights[: 2 * WEIGHT_PARTS]:
+        c.wait()
+
+    def hidden_step(i, carry):
+        columns = pl.ds(pl.multiple_of(i * COLUMNS, COLUMNS), COLUMNS)
+        gate_value = dot(expert_in[...], wg[:, columns])
+        up_value = dot(expert_in[...], wu[:, columns])
+        silu = gate_value / (1.0 + jnp.exp(-gate_value))
+        hidden[:, columns] = (silu * up_value * my_gate).astype(jnp.bfloat16)
+        return carry
+
+    lax.fori_loop(0, ff_share // COLUMNS, hidden_step, 0)
+
+    for c in weights[2 * WEIGHT_PARTS :]:
+        c.wait()
+
+    step = width // DOWN_PARTS
+    for part in range(DOWN_PARTS):
+        partial = dot(hidden[...], wd[:, part * step : (part + 1) * step])
+        for peer in range(n):
+            s5[part, peer] = partial[peer * rows : (peer + 1) * rows].astype(jnp.bfloat16)
+        for d in range(1, n):
+            send(4 + part, d, s5.at[part, lax.rem(me + d, n)], r5.at[part, me])
+        r5[part, me] = s5[part, me]
+    for part in range(DOWN_PARTS):
+        for d in range(1, n):
+            arrive(4 + part, d, lambda source: r5.at[part, source])
+        total = own_mixed[:, part * step : (part + 1) * step]
+        for peer in range(n):
+            total = total + r5[part, peer].astype(jnp.float32)
+        out_ref[:, part * step : (part + 1) * step] = total.astype(jnp.bfloat16)
+    for copy in sent:
+        copy.wait_send()
+
+
+def local(
+    n,
+    tokens,
+    lengths,
+    cache_key,
+    cache_value,
+    routes,
+    route_logits,
+    mix_gain,
+    query_gain,
+    key_gain,
+    head_bias,
+    w_query,
+    w_key,
+    w_value,
+    w_out,
+    ffn_gain,
+    w_gate,
+    w_up,
+    w_down,
+):
+    rows, width = tokens.shape
+    all_rows = rows * n
+    share = width // n
+    q_width, k_width = w_query.shape[1], w_key.shape[1]
+    wide = q_width + k_width + w_value.shape[1]
+    stages = 4 + DOWN_PARTS
+    vmem, anywhere = pl.BlockSpec(memory_space=pltpu.VMEM), pl.BlockSpec(memory_space=pl.ANY)
+    smem = pl.BlockSpec(memory_space=pltpu.SMEM)
+    bf16, f32 = jnp.bfloat16, jnp.float32
+
+    def like(array):
+        return pltpu.VMEM(array.shape, array.dtype)
+
+    flops = 2 * all_rows * 3 * w_gate.shape[0] * w_gate.shape[1]
+    return pl.pallas_call(
+        functools.partial(fused, n),
+        out_shape=(
+            jax.ShapeDtypeStruct((rows, width), bf16),
+            jax.ShapeDtypeStruct((rows, k_width), bf16),
+            jax.ShapeDtypeStruct((rows, w_value.shape[1]), bf16),
+        ),
+        in_specs=[
+            vmem,
+            smem,
+            anywhere,
+            anywhere,
+            vmem,
+            vmem,
+            vmem,
+            vmem,
+            vmem,
+            vmem,
+            anywhere,
+            anywhere,
+            anywhere,
+            anywhere,
+            vmem,
+            anywhere,
+            anywhere,
+            anywhere,
+        ],
+        out_specs=(vmem, vmem, vmem),
+        scratch_shapes=[
+            like(w_query),
+            like(w_key),
+            like(w_value),
+            like(w_out),
+            like(cache_key),
+            like(cache_value),
+            like(w_gate),
+            like(w_up),
+            like(w_down),
+            pltpu.VMEM((n, 2 * rows, share), bf16),
+            pltpu.VMEM((n, 2 * rows, share), bf16),
+            pltpu.VMEM((n, rows, wide), bf16),
+            pltpu.VMEM((n, rows, wide), bf16),
+            pltpu.VMEM((n, rows, q_width), bf16),
+            pltpu.VMEM((n, all_rows, share), bf16),
+            pltpu.VMEM((DOWN_PARTS, n, rows, width // DOWN_PARTS), bf16),
+            pltpu.VMEM((DOWN_PARTS, n, rows, width // DOWN_PARTS), bf16),
+            pltpu.VMEM((all_rows, share), f32),
+            pltpu.VMEM((all_rows, share), f32),
+            pltpu.VMEM((all_rows, q_width), f32),
+            pltpu.VMEM((all_rows, width), bf16),
+            pltpu.VMEM((all_rows, w_gate.shape[1]), bf16),
+            pltpu.SemaphoreType.DMA((4,)),
+            pltpu.SemaphoreType.DMA((rows,)),
+            pltpu.SemaphoreType.DMA((rows,)),
+            pltpu.SemaphoreType.DMA((3, WEIGHT_PARTS)),
+            pltpu.SemaphoreType.DMA((stages, n)),
+            pltpu.SemaphoreType.DMA((stages, n)),
+        ],
+        compiler_params=pltpu.CompilerParams(
+            collective_id=0, has_side_effects=True, vmem_limit_bytes=60 * 1024 * 1024
+        ),
+        cost_estimate=pl.CostEstimate(flops=flops, bytes_accessed=flops // all_rows, transcendentals=0),
+    )(
+        tokens,
+        lengths,
+        cache_key,
+        cache_value,
+        routes,
+        route_logits,
+        mix_gain.reshape(1, -1),
+        query_gain.reshape(1, -1),
+        key_gain.reshape(1, -1),
+        head_bias.reshape(-1, 1),
+        w_query,
+        w_key,
+        w_value,
+        w_out,
+        ffn_gain.reshape(1, -1),
+        w_gate,
+        w_up,
+        w_down,
+    )
+
+
 def solution(mesh):
+    n = mesh.shape["ep"]
+
+    def body(*arrays):
+        tokens, w_gate = arrays[0], arrays[15]
+        share = tokens.shape[1] // n
+        if share == 128 and w_gate.shape[1] % COLUMNS == 0:
+            return local(n, *arrays)
+        return plain(*arrays)
+
     return jax.shard_map(
-        local,
+        body,
         mesh=mesh,
         in_specs=(
             P(("grp", "ep"), None),

time: 324 us -> 57.5 us (0.18)
  waiting for transfers between devices: 144 us -> 0 us
  other arithmetic: 87 us -> 0 us
  Pallas kernels: 0 us -> 48.7 us
  blocking collectives: 42.8 us -> 0 us
  matrix products: 25.7 us -> 0 us
  between operations: 14.6 us -> 0.64 us
    unnamed x6 -> x0, waiting for transfers between devices: 88 us -> none
    another operation x3 -> x0, other arithmetic: 82.2 us -> none
    all_gather x4 -> x0, waiting for transfers between devices: 55.9 us -> none  [the longest x1 49.7 us: local(): lax.all_gather(w_query, 'ep', axis=0, tiled=True)]
    pallas_call x0 -> x1, Pallas kernels: none -> 48.7 us  [local(): pl.pallas_call(functools.partial(fused, n), out_shape=(jax.ShapeDtypeStru...]
    all_gather x2 -> x0, blocking collectives: 42.8 us -> none  [the longest x1 23.2 us: local(): lax.all_gather(route_weights(routes, route_logits), 'ep', axis=0, tiled=T...]
    dot_general x8 -> x0, matrix products: 25.7 us -> none  [the longest x1 8.67 us: local(): jnp.dot(hidden, w_down, preferred_element_type=jnp.float32)]
    unnamed x23 -> x5, local copies, waits for them, and re-layouts: 7.29 us -> 6.48 us
  transfers between devices with their start and end apart: 5 -> 0, of which waited for: 3 -> 0; matrix products, arithmetic and copies ran while one was open for 37% -> 0% of each run, Pallas kernels for 0% -> 0%
where the time goes in v1:
time: 57.5 us; the launch traced here: 57.1 us
  Pallas kernels  48.7 us (85%)
  local copies, waits for them, and re-layouts  7.81 us (14%)
  between operations  0.64 us (1%)
    pallas_call x1, Pallas kernels, local(): pl.pallas_call(functools.partial(fused, n), out_shape=(jax.ShapeDtypeStru...  48.7 us
    unnamed x5, local copies, waits for them, and re-layouts  6.48 us
    reshape x1, local copies, waits for them, and re-layouts, local(): head_bias.reshape(-1, 1)  1.33 us

profile of v1, /device:TPU:0, one launch (start us, length us, event | category | flops | bytes accessed | tf_op | source)
XLA Modules:
  0.0 57.1 jit_solution(10400246984354967729)
XLA Ops:
  0.6 1.3 %copy.21.routes_ref = s32[4,2]{1,0:T(4,128)} copy(s32[4,2]{0,1:T(2,128)} %param.22) | data formatting | bytes 64 | tf_op args[4]
  2.0 1.3 %copy.22.logits_ref = f32[4,2]{1,0:T(4,128)} copy(f32[4,2]{0,1:T(2,128)} %param.23) | data formatting | bytes 64 | tf_op args[5]
  3.3 1.3 %copy.23.head_bias_ref = f32[16,1]{1,0:T(8,128)} copy(f32[16,1]{0,1:T(1,128)} %bitcast.9) | data formatting | bytes 128 | tf_op jit(solution)/shard_map/reshape | solution.py:573
  4.6 48.7 %shard_map.193 = (bf16[4,2048]{1,0:T(4,128)(2,1)}, bf16[4,256]{1,0:T(4,128)(2,1)}, bf16[4,256]{1,0:T(4,128)(2,1)}) custom-call(bf16[4,2048]{1,0:T(4,128)(2,1)} %tokens_ref.1, s32[4]{0:T(128)} %lengths_ref.1, bf16[4,1024,256]{2,1,0:T(8,128)(2,1)} %ck_hbm.1, bf16[4,1024,256]{2,1,0:T(8,128)(2,1)} %cv_hbm.1, s32[4,2]{1,0:T(4,128)} %copy.21.routes_ref, ...), custom_call_target="tpu_custom_call" | custom-call | flops 1409286144 | bytes 22020096 | tf_op jit(solution)/shard_map/pallas_call | solution.py:501
  53.3 1.3 %copy.27 = bf16[4,2048]{1,0:T(4,128)(2,1)} copy(bf16[4,2048]{1,0:T(4,128)(2,1)} %get-tuple-element.6) | data formatting | bytes 32768
  54.7 1.2 %copy.28 = bf16[4,256]{1,0:T(4,128)(2,1)} copy(bf16[4,256]{1,0:T(4,128)(2,1)} %get-tuple-element.7) | data formatting | bytes 4096
  55.9 1.2 %copy.29 = bf16[4,256]{1,0:T(4,128)(2,1)} copy(bf16[4,256]{1,0:T(4,128)(2,1)} %get-tuple-element.8) | data formatting | bytes 4096

commit v2 on v1

--- a/solution.py
+++ b/solution.py
@@ -117,7 +117,7 @@
     return ((mixed + expert_sum).astype(jnp.bfloat16), new_key, new_value)
 
 
-WEIGHT_PARTS = 4
+WEIGHT_PARTS = 2
 DOWN_PARTS = 4
 COLUMNS = 256
 
@@ -130,26 +130,46 @@
     return lax.broadcasted_iota(jnp.int32, shape, dim)
 
 
+def column(row):
+    square = (row.shape[1], row.shape[1])
+    return jnp.sum(
+        jnp.where(iota(square, 0) == iota(square, 1), jnp.broadcast_to(row, square), 0.0),
+        axis=1,
+        keepdims=True,
+    )
+
+
 def fused(
     n,
-    tokens_ref,
+    tokens_hbm,
     lengths_ref,
     ck_hbm,
     cv_hbm,
+    routes_hbm,
+    logits_hbm,
+    mix_gain_hbm,
+    query_gain_hbm,
+    key_gain_hbm,
+    head_bias_hbm,
+    wq_hbm,
+    wk_hbm,
+    wv_hbm,
+    wo_hbm,
+    ffn_gain_hbm,
+    wg_hbm,
+    wu_hbm,
+    wd_hbm,
+    out_any,
+    new_key_any,
+    new_value_any,
+    tokens_ref,
     routes_ref,
     logits_ref,
     mix_gain_ref,
     query_gain_ref,
     key_gain_ref,
     head_bias_ref,
-    wq_hbm,
-    wk_hbm,
-    wv_hbm,
-    wo_hbm,
     ffn_gain_ref,
-    wg_hbm,
-    wu_hbm,
-    wd_hbm,
     out_ref,
     new_key_ref,
     new_value_ref,
@@ -169,18 +189,25 @@
     r3,
     r4,
     s5,
+    p5,
+    t5,
     r5,
     token_cols,
     aux_rows,
     attended_rows,
     expert_in,
     hidden,
+    operand_sem,
+    result_sem,
     small_sem,
     key_sem,
     value_sem,
     weight_sem,
     send_sem,
     recv_sem,
+    block_sem,
+    pair_send_sem,
+    pair_sem,
 ):
     me = lax.axis_index("ep")
     rows, width = tokens_ref.shape
@@ -194,13 +221,38 @@
     my_expert = me // (FF // ff_share)
 
     barrier = pltpu.get_barrier_semaphore()
+    peer_at = [me]
     for d in range(1, n):
+        bit = d.bit_length() - 1
+        flip = 2**bit * (1 - 2 * ((me // 2**bit) % 2))
+        peer_at.append(peer_at[d - 2**bit] + flip)
+    furthest_first = range(n - 1, 0, -1)
+    core, chip = me % 2, me // 2
+    for d in furthest_first:
         pl.semaphore_signal(
             barrier,
             inc=1,
-            device_id={"ep": lax.rem(me + d, n)},
+            device_id={"ep": peer_at[d]},
             device_id_type=pl.DeviceIdType.MESH,
         )
+
+    operands = [
+        pltpu.make_async_copy(a, b, operand_sem.at[i])
+        for i, (a, b) in enumerate(
+            (
+                (tokens_hbm, tokens_ref),
+                (routes_hbm, routes_ref),
+                (logits_hbm, logits_ref),
+                (mix_gain_hbm, mix_gain_ref),
+                (query_gain_hbm, query_gain_ref),
+                (key_gain_hbm, key_gain_ref),
+                (head_bias_hbm, head_bias_ref),
+                (ffn_gain_hbm, ffn_gain_ref),
+            )
+        )
+    ]
+    for c in operands:
+        c.start()
 
     small = [
         pltpu.make_async_copy(a, b, small_sem.at[i])
@@ -210,8 +262,6 @@
         c.start()
     keys = [pltpu.make_async_copy(ck_hbm.at[b], ck.at[b], key_sem.at[b]) for b in range(rows)]
     values = [pltpu.make_async_copy(cv_hbm.at[b], cv.at[b], value_sem.at[b]) for b in range(rows)]
-    for c in keys + values + small[3:]:
-        c.start()
     weights = []
     for which, (a, b) in enumerate(((wg_hbm, wg), (wu_hbm, wu), (wd_hbm, wd))):
         step = b.shape[0] // WEIGHT_PARTS
@@ -222,43 +272,44 @@
                     a.at[piece], b.at[piece], weight_sem.at[which, part]
                 )
             )
-    for c in weights:
-        c.start()
-
-    sent = []
-
-    def send(stage, d, source, target):
+
+    results = [
+        pltpu.make_async_copy(a, b, result_sem.at[i])
+        for i, (a, b) in enumerate(
+            ((out_ref, out_any), (new_key_ref, new_key_any), (new_value_ref, new_value_any))
+        )
+    ]
+    for c in operands:
+        c.wait()
+
+
+    def send(stage, d, source, target, arrival=None):
         copy = pltpu.make_async_remote_copy(
             src_ref=source,
             dst_ref=target,
-            send_sem=send_sem.at[stage, d],
-            recv_sem=recv_sem.at[stage, me],
-            device_id={"ep": lax.rem(me + d, n)},
+            send_sem=send_sem.at[stage],
+            recv_sem=recv_sem.at[stage] if arrival is None else arrival,
+            device_id={"ep": peer_at[d]},
             device_id_type=pl.DeviceIdType.MESH,
         )
         copy.start()
-        sent.append(copy)
-
-    def arrive(stage, d, target_of):
-        source = lax.rem(me + d, n)
-        pltpu.make_async_remote_copy(
-            src_ref=target_of(source),
-            dst_ref=target_of(source),
-            send_sem=send_sem.at[stage, d],
-            recv_sem=recv_sem.at[stage, source],
-            device_id={"ep": source},
-            device_id_type=pl.DeviceIdType.MESH,
-        ).wait_recv()
+
+    def arrived(sem, blocks):
+        pltpu.make_async_copy(blocks, blocks, sem).wait()
+
+    others = pl.ds(0, n - 1)
+    other_chips = pl.ds(0, n // 2 - 1)
 
     as_float = tokens_ref[...].astype(jnp.float32)
     scale = lax.rsqrt(jnp.mean(as_float * as_float, axis=1, keepdims=True) + EPSILON)
     lane = iota((rows, 128), 1)
-    logit_gap = logits_ref[:, 0:1] - logits_ref[:, 1:2]
+    logit_gap = column(logits_ref[0:1] - logits_ref[1:2])
+    chosen = [column(routes_ref[i : i + 1].astype(jnp.float32)) for i in range(2)]
     first_share = 1.0 / (1.0 + jnp.exp(-logit_gap))
     second_share = 1.0 / (1.0 + jnp.exp(logit_gap))
-    expert_lane = lane % EXPERTS
-    gates = jnp.where(routes_ref[:, 0:1] == expert_lane, first_share, 0.0) + jnp.where(
-        routes_ref[:, 1:2] == expert_lane, second_share, 0.0
+    expert_lane = (lane % EXPERTS).astype(jnp.float32)
+    gates = jnp.where(chosen[0] == expert_lane, first_share, 0.0) + jnp.where(
+        chosen[1] == expert_lane, second_share, 0.0
     )
     aux = jnp.where(lane < 3 * EXPERTS, gates, scale)
     high = aux.astype(jnp.bfloat16).astype(jnp.float32)
@@ -272,13 +323,16 @@
         ).astype(jnp.bfloat16)
         s1[peer] = block
     pl.semaphore_wait(barrier, n - 1)
-    for d in range(1, n):
-        send(0, d, s1.at[lax.rem(me + d, n)], r1.at[me])
+    for d in furthest_first:
+        send(0, d, s1.at[peer_at[d]], r1.at[me])
+    for c in keys + values + small[3:]:
+        c.start()
     r1[me] = s1[me]
     for c in small[:3]:
         c.wait()
-    for d in range(1, n):
-        arrive(0, d, lambda source: r1.at[source])
+    arrived(recv_sem.at[0], r1.at[others])
+    for c in weights:
+        c.start()
     for peer in range(n):
         block = r1[peer].astype(jnp.float32)
         token_cols[peer * rows : (peer + 1) * rows, :] = block[:rows]
@@ -302,8 +356,8 @@
             s2[peer, :, start : start + weight.shape[1]] = partial[
                 peer * rows : (peer + 1) * rows
             ].astype(jnp.bfloat16)
-    for d in range(1, n):
-        send(1, d, s2.at[lax.rem(me + d, n)], r2.at[me])
+    for d in furthest_first:
+        send(1, d, s2.at[peer_at[d]], r2.at[me])
     r2[me] = s2[me]
 
     head_of_lane = iota((HEADS, q_width), 1) // HEAD_DIM
@@ -322,8 +376,7 @@
     query_gain = jnp.concatenate([query_gain_ref[...]] * HEADS, axis=1)
     key_gain = jnp.concatenate([key_gain_ref[...]] * KV_HEADS, axis=1)
 
-    for d in range(1, n):
-        arrive(1, d, lambda source: r2.at[source])
+    arrived(recv_sem.at[1], r2.at[others])
     total = r2[0].astype(jnp.float32)
     for peer in range(1, n):
         total = total + r2[peer].astype(jnp.float32)
@@ -338,6 +391,9 @@
         key_scale = jnp.where(key_lane == g, lax.rsqrt(mean + EPSILON), key_scale)
     new_key_ref[...] = (fresh_key * key_scale * key_gain).astype(jnp.bfloat16)
 
+    for c in results[1:]:
+        c.start()
+
     spread = []
     for b in range(rows):
         wide = jnp.where(own_lane, jnp.broadcast_to(queries[b : b + 1], own_lane.shape), 0.0)
@@ -347,6 +403,7 @@
     blocks = cache_len // COLUMNS
     position = iota((HEADS, cache_len), 1)
     own_group = iota((HEADS, k_width), 1) // HEAD_DIM == iota((HEADS, k_width), 0) // group_size
+    head_bias = column(head_bias_ref[...])
     heads = []
     for b in range(rows):
         keys[b].wait()
@@ -356,7 +413,7 @@
             (((1,), (1,)), ((), ())),
             preferred_element_type=jnp.float32,
         ) * HEAD_DIM ** (-0.5)
-        scores = scores + head_bias_ref[...]
+        scores = scores + head_bias
         live = position < lengths_ref[b]
         tail_log = jnp.log1p(jnp.exp(-jnp.abs(scores)))
         remain = jnp.where(live, jnp.minimum(-scores, 0.0) - tail_log, 0.0)
@@ -396,20 +453,25 @@
     ]
     r3[me] = jnp.concatenate(attended, axis=0).astype(jnp.bfloat16)
 
-    for d in range(1, n):
+    for d in furthest_first:
         send(2, d, r3.at[me], r3.at[me])
     small[3].wait()
-    for d in range(1, n):
-        arrive(2, d, lambda source: r3.at[source])
+    arrived(recv_sem.at[2], r3.at[others])
     for peer in range(n):
         attended_rows[peer * rows : (peer + 1) * rows, :] = r3[peer].astype(jnp.float32)
     mixed = token_cols[...] + dot(attended_rows[...].astype(jnp.bfloat16), wo[...])
     r4[me] = mixed.astype(jnp.bfloat16)
 
-    for d in range(1, n):
-        send(3, d, r4.at[me], r4.at[me])
-    for d in range(1, n):
-        arrive(3, d, lambda source: r4.at[source])
+    for d in range(n - 2, 0, -2):
+        send(3, d, r4.at[me], r4.at[me], block_sem.at[me])
+    send(3, 1, r4.at[me], r4.at[me], block_sem.at[me])
+    for d in range(2, n, 2):
+        source = peer_at[d]
+        arrived(block_sem.at[source], r4.at[source])
+        send(3, 1, r4.at[source], r4.at[source], block_sem.at[source])
+    for d in range(1, n, 2):
+        source = peer_at[d]
+        arrived(block_sem.at[source], r4.at[source])
     squares = jnp.zeros((all_rows, share), jnp.float32)
     for peer in range(n):
         block = r4[peer].astype(jnp.float32)
@@ -445,22 +507,51 @@
         c.wait()
 
     step = width // DOWN_PARTS
+
+    pairs = []
+
+    def spread_sums(part):
+        arrived(pair_sem.at[part], p5.at[part])
+        both = s5[part, core].astype(jnp.float32) + p5[part].astype(jnp.float32)
+        t5[part] = both.astype(jnp.bfloat16)
+        for d in range(n - 2, 0, -2):
+            send(4 + part, d, t5.at[part, peer_at[d] // 2], r5.at[part, chip])
+        r5[part, chip] = t5[part, chip]
+
     for part in range(DOWN_PARTS):
         partial = dot(hidden[...], wd[:, part * step : (part + 1) * step])
         for peer in range(n):
-            s5[part, peer] = partial[peer * rows : (peer + 1) * rows].astype(jnp.bfloat16)
-        for d in range(1, n):
-            send(4 + part, d, s5.at[part, lax.rem(me + d, n)], r5.at[part, me])
-        r5[part, me] = s5[part, me]
+            s5[part, peer % 2, peer // 2] = partial[peer * rows : (peer + 1) * rows].astype(
+                jnp.bfloat16
+            )
+        pairs.append(
+            pltpu.make_async_remote_copy(
+                src_ref=s5.at[part, 1 - core],
+                dst_ref=p5.at[part],
+                send_sem=pair_send_sem.at[part],
+                recv_sem=pair_sem.at[part],
+                device_id={"ep": peer_at[1]},
+                device_id_type=pl.DeviceIdType.MESH,
+            )
+        )
+        pairs[-1].start()
+        if part:
+            spread_sums(part - 1)
+    spread_sums(DOWN_PARTS - 1)
     for part in range(DOWN_PARTS):
-        for d in range(1, n):
-            arrive(4 + part, d, lambda source: r5.at[part, source])
+        arrived(recv_sem.at[4 + part], r5.at[part, other_chips])
         total = own_mixed[:, part * step : (part + 1) * step]
-        for peer in range(n):
+        for peer in range(n // 2):
             total = total + r5[part, peer].astype(jnp.float32)
         out_ref[:, part * step : (part + 1) * step] = total.astype(jnp.bfloat16)
-    for copy in sent:
-        copy.wait_send()
+    results[0].start()
+    for stage, blocks in enumerate((s1, s2, r3, r4)):
+        arrived(send_sem.at[stage], blocks.at[others])
+    for part in range(DOWN_PARTS):
+        pairs[part].wait_send()
+        arrived(send_sem.at[4 + part], t5.at[part, other_chips])
+    for c in results:
+        c.wait()
 
 
 def local(
@@ -490,7 +581,7 @@
     q_width, k_width = w_query.shape[1], w_key.shape[1]
     wide = q_width + k_width + w_value.shape[1]
     stages = 4 + DOWN_PARTS
-    vmem, anywhere = pl.BlockSpec(memory_space=pltpu.VMEM), pl.BlockSpec(memory_space=pl.ANY)
+    anywhere = pl.BlockSpec(memory_space=pl.ANY)
     smem = pl.BlockSpec(memory_space=pltpu.SMEM)
     bf16, f32 = jnp.bfloat16, jnp.float32
 
@@ -498,35 +589,22 @@
         return pltpu.VMEM(array.shape, array.dtype)
 
     flops = 2 * all_rows * 3 * w_gate.shape[0] * w_gate.shape[1]
+    shapes = ((rows, width), (rows, k_width), (rows, w_value.shape[1]))
     return pl.pallas_call(
         functools.partial(fused, n),
-        out_shape=(
-            jax.ShapeDtypeStruct((rows, width), bf16),
-            jax.ShapeDtypeStruct((rows, k_width), bf16),
-            jax.ShapeDtypeStruct((rows, w_value.shape[1]), bf16),
-        ),
-        in_specs=[
-            vmem,
-            smem,
-            anywhere,
-            anywhere,
-            vmem,
-            vmem,
-            vmem,
-            vmem,
-            vmem,
-            vmem,
-            anywhere,
-            anywhere,
-            anywhere,
-            anywhere,
-            vmem,
-            anywhere,
-            anywhere,
-            anywhere,
-        ],
-        out_specs=(vmem, vmem, vmem),
+        out_shape=tuple(pltpu.VMEM(shape, bf16) for shape in shapes),
+        in_specs=[anywhere, smem] + [anywhere] * 16,
+        out_specs=(anywhere,) * 3,
         scratch_shapes=[
+            like(tokens),
+            pltpu.VMEM(routes.shape[::-1], routes.dtype),
+            pltpu.VMEM(route_logits.shape[::-1], f32),
+            pltpu.VMEM((1, width), f32),
+            pltpu.VMEM((1, HEAD_DIM), f32),
+            pltpu.VMEM((1, HEAD_DIM), f32),
+            pltpu.VMEM((1, HEADS), f32),
+            pltpu.VMEM((1, width), f32),
+            *(pltpu.VMEM(shape, bf16) for shape in shapes),
             like(w_query),
             like(w_key),
             like(w_value),
@@ -542,19 +620,26 @@
             pltpu.VMEM((n, rows, wide), bf16),
             pltpu.VMEM((n, rows, q_width), bf16),
             pltpu.VMEM((n, all_rows, share), bf16),
-            pltpu.VMEM((DOWN_PARTS, n, rows, width // DOWN_PARTS), bf16),
-            pltpu.VMEM((DOWN_PARTS, n, rows, width // DOWN_PARTS), bf16),
+            pltpu.VMEM((DOWN_PARTS, 2, n // 2, rows, width // DOWN_PARTS), bf16),
+            pltpu.VMEM((DOWN_PARTS, n // 2, rows, width // DOWN_PARTS), bf16),
+            pltpu.VMEM((DOWN_PARTS, n // 2, rows, width // DOWN_PARTS), bf16),
+            pltpu.VMEM((DOWN_PARTS, n // 2, rows, width // DOWN_PARTS), bf16),
             pltpu.VMEM((all_rows, share), f32),
             pltpu.VMEM((all_rows, share), f32),
             pltpu.VMEM((all_rows, q_width), f32),
             pltpu.VMEM((all_rows, width), bf16),
             pltpu.VMEM((all_rows, w_gate.shape[1]), bf16),
+            pltpu.SemaphoreType.DMA((8,)),
+            pltpu.SemaphoreType.DMA((3,)),
             pltpu.SemaphoreType.DMA((4,)),
             pltpu.SemaphoreType.DMA((rows,)),
             pltpu.SemaphoreType.DMA((rows,)),
             pltpu.SemaphoreType.DMA((3, WEIGHT_PARTS)),
-            pltpu.SemaphoreType.DMA((stages, n)),
-            pltpu.SemaphoreType.DMA((stages, n)),
+            pltpu.SemaphoreType.DMA((stages,)),
+            pltpu.SemaphoreType.DMA((stages,)),
+            pltpu.SemaphoreType.DMA((n,)),
+            pltpu.SemaphoreType.DMA((DOWN_PARTS,)),
+            pltpu.SemaphoreType.DMA((DOWN_PARTS,)),
         ],
         compiler_params=pltpu.CompilerParams(
             collective_id=0, has_side_effects=True, vmem_limit_bytes=60 * 1024 * 1024
@@ -565,12 +650,12 @@
         lengths,
         cache_key,
         cache_value,
-        routes,
-        route_logits,
+        routes.T,
+        route_logits.T,
         mix_gain.reshape(1, -1),
         query_gain.reshape(1, -1),
         key_gain.reshape(1, -1),
-        head_bias.reshape(-1, 1),
+        head_bias.reshape(1, -1),
         w_query,
         w_key,
         w_value,
@@ -588,7 +673,7 @@
     def body(*arrays):
         tokens, w_gate = arrays[0], arrays[15]
         share = tokens.shape[1] // n
-        if share == 128 and w_gate.shape[1] % COLUMNS == 0:
+        if share == 128 and n & (n - 1) == 0 and w_gate.shape[1] % COLUMNS == 0:
             return local(n, *arrays)
         return plain(*arrays)
 

time: 57.5 us -> 45.3 us (0.79)
  Pallas kernels: 48.7 us -> 42.6 us
  local copies, waits for them, and re-layouts: 7.81 us -> 1.76 us
    pallas_call x1, Pallas kernels: 48.7 us -> 42.6 us  [local(): pl.pallas_call(functools.partial(fused, n), out_shape=tuple((pltpu.VMEM(s...]
    unnamed x5 -> x3, local copies, waits for them, and re-layouts: 6.48 us -> 1.76 us
    reshape x1 -> x0, local copies, waits for them, and re-layouts: 1.33 us -> none  [local(): head_bias.reshape(-1, 1)]
where the time goes in v2:
time: 45.3 us; the launch traced here: 45 us
  Pallas kernels  42.6 us (94%)
  local copies, waits for them, and re-layouts  1.76 us (4%)
  between operations  0.65 us (1%)
    pallas_call x1, Pallas kernels, local(): pl.pallas_call(functools.partial(fused, n), out_shape=tuple((pltpu.VMEM(s...  42.6 us
    unnamed x3, local copies, waits for them, and re-layouts  1.76 us

profile of v2, /device:TPU:0, one launch (start us, length us, event | category | flops | bytes accessed | tf_op | source)
XLA Modules:
  0.0 45.0 jit_solution(10894344739944248146)
XLA Ops:
  0.6 42.6 %shard_map.193 = (bf16[4,2048]{1,0:T(4,128)(2,1)S(1)}, bf16[4,256]{1,0:T(4,128)(2,1)S(1)}, bf16[4,256]{1,0:T(4,128)(2,1)S(1)}) custom-call(bf16[4,2048]{1,0:T(4,128)(2,1)} %tokens_hbm.1, s32[4]{0:T(128)} %lengths_ref.1, bf16[4,1024,256]{2,1,0:T(8,128)(2,1)} %ck_hbm.1, bf16[4,1024,256]{2,1,0:T(8,128)(2,1)} %cv_hbm.1, s32[2,4]{1,0:T(2,128)} %bitcast.9, ...), custom_call_target="tpu_custom_call" | custom-call | flops 1409286144 | bytes 22020096 | tf_op jit(solution)/shard_map/pallas_call | solution.py:593
  43.2 0.6 %copy.24 = bf16[4,2048]{1,0:T(4,128)(2,1)} copy(bf16[4,2048]{1,0:T(4,128)(2,1)S(1)} %get-tuple-element.3) | data formatting | bytes 32768
  43.8 0.6 %copy.25 = bf16[4,256]{1,0:T(4,128)(2,1)} copy(bf16[4,256]{1,0:T(4,128)(2,1)S(1)} %get-tuple-element.4) | data formatting | bytes 4096
  44.4 0.6 %copy.26 = bf16[4,256]{1,0:T(4,128)(2,1)} copy(bf16[4,256]{1,0:T(4,128)(2,1)S(1)} %get-tuple-element.5) | data formatting | bytes 4096

commit v3 on v2

--- a/solution.py
+++ b/solution.py
@@ -185,6 +185,8 @@
     s1,
     r1,
     s2,
+    p2,
+    t2,
     r2,
     r3,
     r4,
@@ -353,12 +355,18 @@
     for weight, start in ((wq, 0), (wk, q_width), (wv, q_width + k_width)):
         partial = dot(normed, weight[...])
         for peer in range(n):
-            s2[peer, :, start : start + weight.shape[1]] = partial[
+            s2[peer % 2, peer // 2, :, start : start + weight.shape[1]] = partial[
                 peer * rows : (peer + 1) * rows
             ].astype(jnp.bfloat16)
-    for d in furthest_first:
-        send(1, d, s2.at[peer_at[d]], r2.at[me])
-    r2[me] = s2[me]
+    pair = pltpu.make_async_remote_copy(
+        src_ref=s2.at[1 - core],
+        dst_ref=p2,
+        send_sem=pair_send_sem.at[DOWN_PARTS],
+        recv_sem=pair_sem.at[DOWN_PARTS],
+        device_id={"ep": peer_at[1]},
+        device_id_type=pl.DeviceIdType.MESH,
+    )
+    pair.start()
 
     head_of_lane = iota((HEADS, q_width), 1) // HEAD_DIM
     own_lane = head_of_lane == iota((HEADS, q_width), 0)
@@ -376,9 +384,14 @@
     query_gain = jnp.concatenate([query_gain_ref[...]] * HEADS, axis=1)
     key_gain = jnp.concatenate([key_gain_ref[...]] * KV_HEADS, axis=1)
 
-    arrived(recv_sem.at[1], r2.at[others])
+    pair.wait_recv()
+    t2[...] = (s2[core].astype(jnp.float32) + p2[...].astype(jnp.float32)).astype(jnp.bfloat16)
+    for d in range(n - 2, 0, -2):
+        send(1, d, t2.at[peer_at[d] // 2], r2.at[chip])
+    r2[chip] = t2[chip]
+    arrived(recv_sem.at[1], r2.at[other_chips])
     total = r2[0].astype(jnp.float32)
-    for peer in range(1, n):
+    for peer in range(1, n // 2):
         total = total + r2[peer].astype(jnp.float32)
     queries = total[:, :q_width]
     fresh_key = total[:, q_width : q_width + k_width]
@@ -401,46 +414,51 @@
         spread.append((wide * lax.rsqrt(mean + EPSILON) * query_gain).astype(jnp.bfloat16))
     folded = dot(jnp.concatenate(spread, axis=0), fold).astype(jnp.bfloat16)
     blocks = cache_len // COLUMNS
-    position = iota((HEADS, cache_len), 1)
-    own_group = iota((HEADS, k_width), 1) // HEAD_DIM == iota((HEADS, k_width), 0) // group_size
-    head_bias = column(head_bias_ref[...])
-    heads = []
+    head_rows = rows * HEADS
+    head_bias = jnp.concatenate([column(head_bias_ref[...])] * rows, axis=0)
+    row_of = iota((head_rows, 1), 0) // HEADS
+    lengths = jnp.zeros((head_rows, 1), jnp.int32)
     for b in range(rows):
-        keys[b].wait()
-        scores = lax.dot_general(
-            folded[b * HEADS : (b + 1) * HEADS],
-            ck[b],
-            (((1,), (1,)), ((), ())),
-            preferred_element_type=jnp.float32,
-        ) * HEAD_DIM ** (-0.5)
-        scores = scores + head_bias
-        live = position < lengths_ref[b]
-        tail_log = jnp.log1p(jnp.exp(-jnp.abs(scores)))
-        remain = jnp.where(live, jnp.minimum(-scores, 0.0) - tail_log, 0.0)
-        stacked = jnp.concatenate(
-            [remain[:, i * COLUMNS : (i + 1) * COLUMNS] for i in range(blocks)], axis=0
-        )
-        high = stacked.astype(jnp.bfloat16)
-        rest = stacked - high.astype(jnp.float32)
-        middle = rest.astype(jnp.bfloat16)
-        low = (rest - middle.astype(jnp.float32)).astype(jnp.bfloat16)
-        sums = dot(jnp.concatenate([high, middle, low], axis=0), later)
-        count = blocks * HEADS
-        sums = sums[:count] + sums[count : 2 * count] + sums[2 * count :]
-        totals = jnp.sum(stacked, axis=1, keepdims=True)
-        after = [None] * blocks
-        carry = jnp.zeros((HEADS, 1), jnp.float32)
-        for i in reversed(range(blocks)):
-            after[i] = sums[i * HEADS : (i + 1) * HEADS] + carry
-            carry = carry + totals[i * HEADS : (i + 1) * HEADS]
-        after_sum = jnp.concatenate(after, axis=1)
-        chance = jnp.exp(jnp.minimum(scores, 0.0) - tail_log + after_sum)
-        weight = jnp.where(live, chance, 0.0).astype(jnp.bfloat16)
-        values[b].wait()
-        mixed_heads = dot(weight, cv[b])
-        heads.append(jnp.where(own_group, mixed_heads, 0.0).astype(jnp.bfloat16))
+        lengths = jnp.where(row_of == b, lengths_ref[b], lengths)
+    live = iota((head_rows, cache_len), 1) < lengths
+    for c in keys + values:
+        c.wait()
+    scores = jnp.concatenate(
+        [
+            lax.dot_general(
+                folded[b * HEADS : (b + 1) * HEADS],
+                ck[b],
+                (((1,), (1,)), ((), ())),
+                preferred_element_type=jnp.float32,
+            )
+            for b in range(rows)
+        ],
+        axis=0,
+    )
+    scores = scores * HEAD_DIM ** (-0.5) + head_bias
+    tail_log = jnp.log1p(jnp.exp(-jnp.abs(scores)))
+    remain = jnp.where(live, jnp.minimum(-scores, 0.0) - tail_log, 0.0)
+    after = [None] * blocks
+    carry = jnp.zeros((head_rows, 1), jnp.float32)
+    for i in reversed(range(blocks)):
+        block = remain[:, i * COLUMNS : (i + 1) * COLUMNS]
+        high = block.astype(jnp.bfloat16)
+        low = (block - high.astype(jnp.float32)).astype(jnp.bfloat16)
+        after[i] = dot(high, later) + dot(low, later) + carry
+        carry = carry + jnp.sum(block, axis=1, keepdims=True)
+    after_sum = jnp.concatenate(after, axis=1)
+    chance = jnp.exp(jnp.minimum(scores, 0.0) - tail_log + after_sum)
+    weight = jnp.where(live, chance, 0.0).astype(jnp.bfloat16)
+    mixed_heads = jnp.concatenate(
+        [dot(weight[b * HEADS : (b + 1) * HEADS], cv[b]) for b in range(rows)], axis=0
+    )
+    own_group = (
+        iota((head_rows, k_width), 1) // HEAD_DIM
+        == iota((head_rows, k_width), 0) % HEADS // group_size
+    )
+    heads = jnp.where(own_group, mixed_heads, 0.0).astype(jnp.bfloat16)
     unfolded = lax.dot_general(
-        jnp.concatenate(heads, axis=0),
+        heads,
         fold,
         (((1,), (1,)), ((), ())),
         preferred_element_type=jnp.float32,
@@ -545,8 +563,11 @@
             total = total + r5[part, peer].astype(jnp.float32)
         out_ref[:, part * step : (part + 1) * step] = total.astype(jnp.bfloat16)
     results[0].start()
-    for stage, blocks in enumerate((s1, s2, r3, r4)):
-        arrived(send_sem.at[stage], blocks.at[others])
+    for stage, blocks in enumerate((s1, None, r3, r4)):
+        if blocks is not None:
+            arrived(send_sem.at[stage], blocks.at[others])
+    arrived(send_sem.at[1], t2.at[other_chips])
+    pair.wait_send()
     for part in range(DOWN_PARTS):
         pairs[part].wait_send()
         arrived(send_sem.at[4 + part], t5.at[part, other_chips])
@@ -616,8 +637,10 @@
             like(w_down),
             pltpu.VMEM((n, 2 * rows, share), bf16),
             pltpu.VMEM((n, 2 * rows, share), bf16),
-            pltpu.VMEM((n, rows, wide), bf16),
-            pltpu.VMEM((n, rows, wide), bf16),
+            pltpu.VMEM((2, n // 2, rows, wide), bf16),
+            pltpu.VMEM((n // 2, rows, wide), bf16),
+            pltpu.VMEM((n // 2, rows, wide), bf16),
+            pltpu.VMEM((n // 2, rows, wide), bf16),
             pltpu.VMEM((n, rows, q_width), bf16),
             pltpu.VMEM((n, all_rows, share), bf16),
             pltpu.VMEM((DOWN_PARTS, 2, n // 2, rows, width // DOWN_PARTS), bf16),
@@ -638,8 +661,8 @@
             pltpu.SemaphoreType.DMA((stages,)),
             pltpu.SemaphoreType.DMA((stages,)),
             pltpu.SemaphoreType.DMA((n,)),
-            pltpu.SemaphoreType.DMA((DOWN_PARTS,)),
-            pltpu.SemaphoreType.DMA((DOWN_PARTS,)),
+            pltpu.SemaphoreType.DMA((DOWN_PARTS + 1,)),
+            pltpu.SemaphoreType.DMA((DOWN_PARTS + 1,)),
         ],
         compiler_params=pltpu.CompilerParams(
             collective_id=0, has_side_effects=True, vmem_limit_bytes=60 * 1024 * 1024

time: 45.3 us -> 42.9 us (0.947)
  Pallas kernels: 42.6 us -> 40.2 us
    pallas_call x1, Pallas kernels: 42.6 us -> 40.2 us  [local(): pl.pallas_call(functools.partial(fused, n), out_shape=tuple((pltpu.VMEM(s...]
where the time goes in v3:
time: 42.9 us; the launch traced here: 42.6 us
  Pallas kernels  40.2 us (94%)
  local copies, waits for them, and re-layouts  1.76 us (4%)
  between operations  0.65 us (2%)
    pallas_call x1, Pallas kernels, local(): pl.pallas_call(functools.partial(fused, n), out_shape=tuple((pltpu.VMEM(s...  40.2 us
    unnamed x3, local copies, waits for them, and re-layouts  1.76 us

profile of v3, /device:TPU:0, one launch (start us, length us, event | category | flops | bytes accessed | tf_op | source)
XLA Modules:
  0.0 42.6 jit_solution(17135569916068379661)
XLA Ops:
  0.6 40.2 %shard_map.193 = (bf16[4,2048]{1,0:T(4,128)(2,1)S(1)}, bf16[4,256]{1,0:T(4,128)(2,1)S(1)}, bf16[4,256]{1,0:T(4,128)(2,1)S(1)}) custom-call(bf16[4,2048]{1,0:T(4,128)(2,1)} %tokens_hbm.1, s32[4]{0:T(128)} %lengths_ref.1, bf16[4,1024,256]{2,1,0:T(8,128)(2,1)} %ck_hbm.1, bf16[4,1024,256]{2,1,0:T(8,128)(2,1)} %cv_hbm.1, s32[2,4]{1,0:T(2,128)} %bitcast.9, ...), custom_call_target="tpu_custom_call" | custom-call | flops 1409286144 | bytes 22020096 | tf_op jit(solution)/shard_map/pallas_call | solution.py:614
  40.8 0.6 %copy.24 = bf16[4,2048]{1,0:T(4,128)(2,1)} copy(bf16[4,2048]{1,0:T(4,128)(2,1)S(1)} %get-tuple-element.3) | data formatting | bytes 32768
  41.4 0.6 %copy.25 = bf16[4,256]{1,0:T(4,128)(2,1)} copy(bf16[4,256]{1,0:T(4,128)(2,1)S(1)} %get-tuple-element.4) | data formatting | bytes 4096
  42.0 0.6 %copy.26 = bf16[4,256]{1,0:T(4,128)(2,1)} copy(bf16[4,256]{1,0:T(4,128)(2,1)S(1)} %get-tuple-element.5) | data formatting | bytes 4096

commit v4 on v3

--- a/solution.py
+++ b/solution.py
@@ -137,6 +137,17 @@
         axis=1,
         keepdims=True,
     )
+
+
+def finish(*refs):
+    half = len(refs) // 2
+    copies = [
+        pltpu.make_async_copy(refs[i], refs[half + i], refs[-1].at[i]) for i in range(half)
+    ]
+    for copy in copies:
+        copy.start()
+    for copy in copies:
+        copy.wait()
 
 
 def fused(
@@ -611,7 +622,7 @@
 
     flops = 2 * all_rows * 3 * w_gate.shape[0] * w_gate.shape[1]
     shapes = ((rows, width), (rows, k_width), (rows, w_value.shape[1]))
-    return pl.pallas_call(
+    results = pl.pallas_call(
         functools.partial(fused, n),
         out_shape=tuple(pltpu.VMEM(shape, bf16) for shape in shapes),
         in_specs=[anywhere, smem] + [anywhere] * 16,
@@ -688,6 +699,13 @@
         w_up,
         w_down,
     )
+    return pl.pallas_call(
+        finish,
+        out_shape=tuple(jax.ShapeDtypeStruct(shape, bf16) for shape in shapes),
+        in_specs=[anywhere] * len(shapes),
+        out_specs=(anywhere,) * len(shapes),
+        scratch_shapes=[pltpu.SemaphoreType.DMA((len(shapes),))],
+    )(*(pltpu.with_memory_space_constraint(result, pltpu.VMEM) for result in results))
 
 
 def solution(mesh):

time: 42.9 us -> 41.7 us (0.972)
  local copies, waits for them, and re-layouts: 1.76 us -> 0 us
  Pallas kernels: 40.2 us -> 40.8 us
    unnamed x3 -> x0, local copies, waits for them, and re-layouts: 1.76 us -> none
    pallas_call x0 -> x1, Pallas kernels: none -> 0.64 us  [local(): pl.pallas_call(finish, out_shape=tuple((jax.ShapeDtypeStruct(shape, bf16)...]
where the time goes in v4:
time: 41.7 us; the launch traced here: 41.5 us
  Pallas kernels  40.8 us (98%)
  between operations  0.65 us (2%)
    pallas_call x1, Pallas kernels, local(): pl.pallas_call(functools.partial(fused, n), out_shape=tuple((pltpu.VMEM(s...  40.2 us

profile of v4, /device:TPU:0, one launch (start us, length us, event | category | flops | bytes accessed | tf_op | source)
XLA Modules:
  0.0 41.5 jit_solution(15267929637288289584)
XLA Ops:
  0.6 40.2 %shard_map.193 = (bf16[4,2048]{1,0:T(4,128)(2,1)S(1)}, bf16[4,256]{1,0:T(4,128)(2,1)S(1)}, bf16[4,256]{1,0:T(4,128)(2,1)S(1)}) custom-call(bf16[4,2048]{1,0:T(4,128)(2,1)} %tokens_hbm.1, s32[4]{0:T(128)} %lengths_ref.1, bf16[4,1024,256]{2,1,0:T(8,128)(2,1)} %ck_hbm.1, bf16[4,1024,256]{2,1,0:T(8,128)(2,1)} %cv_hbm.1, s32[2,4]{1,0:T(2,128)} %bitcast.9, ...), custom_call_target="tpu_custom_call" | custom-call | flops 1409286144 | bytes 22020096 | tf_op jit(solution)/shard_map/pallas_call | solution.py:625
  40.8 0.6 %shard_map.194 = (bf16[4,2048]{1,0:T(4,128)(2,1)}, bf16[4,256]{1,0:T(4,128)(2,1)}, bf16[4,256]{1,0:T(4,128)(2,1)}) custom-call(bf16[4,2048]{1,0:T(4,128)(2,1)S(1)} %get-tuple-element.6.refs_0_, bf16[4,256]{1,0:T(4,128)(2,1)S(1)} %get-tuple-element.7.refs_1_, bf16[4,256]{1,0:T(4,128)(2,1)S(1)} %get-tuple-element.8.refs_2_), custom_call_target="tpu_custom_call" | custom-call | tf_op jit(solution)/shard_map/pallas_call | solution.py:702
